TPU v7x, 32 devices: a whole 2x2x4 slice. The times are simulated.
32 devices in a mesh: grp: 2 (over y), sp: 4 (over z), tp: 4 (over x, core).
Axes of the slice: x: 2, y: 2, z: 4, core: 2. Of those that a mesh axis runs over, the one named last changes fastest.
Arguments:
- tokens: bfloat16 [3072, 2048], P(('grp', 'sp'), 'tp'), parts along dimension 0, may hold values from -6 to 6
- norm_gain: float32 [2048], replicated, may hold values from 0.1 to 1.9
- qk_gain: float32 [4, 64], replicated, may hold values from 0.7 to 5.5
- w_query_window: bfloat16 [2048, 1024], P('sp', 'tp'), may hold values from -1 to 1
- w_key_window: bfloat16 [2048, 512], P('sp', 'tp'), may hold values from -1 to 1
- w_value_window: bfloat16 [2048, 512], P('sp', 'tp'), may hold values from -0.125 to 0.125
- sink_logits: float32 [16], P('tp'), may hold values from 0 to 5
- w_query_forget: bfloat16 [2048, 1024], P('sp', 'tp'), may hold values from -1 to 1
- w_key_forget: bfloat16 [2048, 1024], P('sp', 'tp'), may hold values from -1 to 1
- w_value_forget: bfloat16 [2048, 1024], P('sp', 'tp'), may hold values from -0.125 to 0.125
- gate_cum: float32 [3072, 16], P(('grp', 'sp'), 'tp'), parts along dimension 0, as said below
- w_merge: bfloat16 [2048, 2, 2048], P('sp', None, 'tp'), may hold values from -0.125 to 0.125
- w_branch: bfloat16 [2, 1024, 2048], P(None, 'sp', 'tp'), may hold values from -0.8984375 to 0.8984375
Outputs:
- mixed: bfloat16 [3072, 2048], P(('grp', 'sp'), 'tp'), parts along dimension 0
There are 2 independent parts, one for each index of `grp`. A program takes and returns all parts, laid end to end along the dimension named above; an argument that names none is the same for every part. Nothing has to cross between parts.
Inputs may be any that keep to these rules, and one draw needn't show every extreme that they name: `gate_cum`: along positions each head's values never rise.
All inputs are finite; a program needn't handle non-finite values.
Results may differ from a plain program's by a relative error of at most 0.012.
Values may be sent and summed in bfloat16 or wider, within the bound.
A program may use at most 64 MiB of HBM per device.

v0:
```python
import math
import jax
import jax.numpy as jnp
from jax import lax
from jax.sharding import PartitionSpec as P

HEAD = 64
WINDOW = 128
epsilon = 1e-06
big_negative = -1e30


def from_behind(value, axis, by):
    size = lax.axis_size(axis)
    pairs = [(i, i + by) for i in range(size) if 0 <= i + by < size]
    return lax.ppermute(value, axis, pairs)


def head_norm(raw, gain, head_count):
    split = raw.reshape(raw.shape[0], head_count, -1)
    scaled = split * lax.rsqrt(jnp.mean(split * split, axis=-1, keepdims=True) + epsilon) * gain
    return scaled.astype(jnp.bfloat16)


def window_attend(queries, keys_ext, values_ext, sink_rows, first_pos):
    row_count, head_count, head_size = queries.shape
    group_count = keys_ext.shape[1]
    span_rows = WINDOW // 2
    block_count = row_count // span_rows
    query_blocks = queries.reshape(
        block_count, span_rows, group_count, head_count // group_count, head_size
    )
    key_blocks = jnp.concatenate(
        [
            keys_ext[lag_index * span_rows : lag_index * span_rows + row_count].reshape(
                block_count, span_rows, group_count, head_size
            )
            for lag_index in range(3)
        ],
        axis=1,
    )
    value_blocks = jnp.concatenate(
        [
            values_ext[lag_index * span_rows : lag_index * span_rows + row_count].reshape(
                block_count, span_rows, group_count, head_size
            )
            for lag_index in range(3)
        ],
        axis=1,
    )
    scores = jnp.einsum(
        "nqgrd,nkgd->ngrqk", query_blocks, key_blocks, preferred_element_type=jnp.float32
    ) * head_size ** (-0.5)
    distance = WINDOW + jnp.arange(span_rows)[:, None] - jnp.arange(3 * span_rows)[None, :]
    key_pos = (
        first_pos
        - WINDOW
        + jnp.arange(block_count)[:, None] * span_rows
        + jnp.arange(3 * span_rows)[None, :]
    )
    is_valid = ((distance >= 0) & (distance < WINDOW))[None] & (key_pos >= 0)[:, None, :]
    is_valid = is_valid[:, None, None]
    sink_grid = sink_rows.reshape(1, group_count, head_count // group_count, 1)
    row_max = jnp.maximum(jnp.max(jnp.where(is_valid, scores, big_negative), axis=-1), sink_grid)
    weights = jnp.where(is_valid, jnp.exp(scores - row_max[..., None]), 0.0)
    row_total = jnp.sum(weights, axis=-1) + jnp.exp(sink_grid - row_max)
    prob_rows = (weights / row_total[..., None]).astype(jnp.bfloat16)
    mixed_sum = jnp.einsum(
        "ngrqk,nkgd->nqgrd", prob_rows, value_blocks, preferred_element_type=jnp.float32
    )
    return mixed_sum.reshape(row_count, head_count * head_size).astype(jnp.bfloat16)


def forget_groups(groups, keys, values, gates):
    head_count, head_size = (keys.shape[1], keys.shape[2])
    gates_all = lax.all_gather(gates, "sp", axis=0, tiled=True)

    def absorber(queries, query_gate, query_pos):

        def absorb(running, block):
            row_max, row_total, mixed_sum = running
            key_rows, value_rows, key_gate, key_pos = block
            scores = jnp.einsum(
                "qhd,khd->hqk", queries, key_rows, preferred_element_type=jnp.float32
            ) * head_size ** (-0.5)
            scores = scores + query_gate.T[:, :, None] - key_gate.T[:, None, :]
            is_valid = (query_pos[:, None] >= key_pos[None, :])[None]
            new_max = jnp.maximum(
                row_max, jnp.max(jnp.where(is_valid, scores, big_negative), axis=-1)
            )
            weights = jnp.where(is_valid, jnp.exp(scores - new_max[..., None]), 0.0)
            shrink = jnp.exp(row_max - new_max)
            row_total = row_total * shrink + jnp.sum(weights, axis=-1)
            mixed_sum = mixed_sum * shrink.T[:, :, None] + jnp.einsum(
                "hqk,khd->qhd",
                weights.astype(jnp.bfloat16),
                value_rows,
                preferred_element_type=jnp.float32,
            )
            return ((new_max, row_total, mixed_sum), None)

        return absorb

    initial = tuple(
        (
            (
                jnp.full((head_count, group[0].shape[0]), big_negative, jnp.float32),
                jnp.zeros((head_count, group[0].shape[0]), jnp.float32),
                jnp.zeros((group[0].shape[0], head_count, head_size), jnp.float32),
            )
            for group in groups
        )
    )
    first_row = jnp.int32(0)
    key_rows = lax.all_gather(keys, "sp", axis=0, tiled=True)
    value_rows = lax.all_gather(values, "sp", axis=0, tiled=True)
    piece_rows = key_rows.shape[0]
    sub_rows = math.gcd(piece_rows, 2048)
    turns = piece_rows // sub_rows
    key_gate = gates_all
    key_pos = jnp.arange(piece_rows)
    blocks = (
        key_rows.reshape(turns, sub_rows, head_count, head_size),
        value_rows.reshape(turns, sub_rows, head_count, head_size),
        key_gate.reshape(turns, sub_rows, head_count),
        key_pos.reshape(turns, sub_rows),
    )
    updated = []
    for (queries, query_gate, query_pos), state in zip(groups, initial):
        absorb = absorber(queries, query_gate, query_pos)

        def advance(current):
            return lax.scan(absorb, current, blocks)[0]

        def keep(current):
            return current

        updated.append(lax.cond(first_row <= query_pos[-1], advance, keep, state))
    finals = tuple(updated)
    return [
        (mixed_sum / row_total.T[:, :, None])
        .reshape(mixed_sum.shape[0], head_count * head_size)
        .astype(jnp.bfloat16)
        for row_max, row_total, mixed_sum in finals
    ]


def on_device(
    tokens,
    norm_gain,
    qk_gain,
    w_query_window,
    w_key_window,
    w_value_window,
    sink_logits,
    w_query_forget,
    w_key_forget,
    w_value_forget,
    gate_cum,
    w_merge,
    w_branch,
):
    row_count = tokens.shape[0]
    row_offset = lax.axis_index("sp") * row_count
    gathered = lax.all_gather(tokens, "tp", axis=1, tiled=True)
    as_float = gathered.astype(jnp.float32)
    normed = (
        as_float
        * lax.rsqrt(jnp.mean(as_float * as_float, axis=-1, keepdims=True) + epsilon)
        * norm_gain
    ).astype(jnp.bfloat16)
    merge_flat = w_merge.reshape(w_merge.shape[0], -1)
    pieces = (
        lax.all_gather(w_query_window, "sp", axis=0, tiled=True),
        lax.all_gather(w_key_window, "sp", axis=0, tiled=True),
        lax.all_gather(w_value_window, "sp", axis=0, tiled=True),
        lax.all_gather(w_query_forget, "sp", axis=0, tiled=True),
        lax.all_gather(w_key_forget, "sp", axis=0, tiled=True),
        lax.all_gather(w_value_forget, "sp", axis=0, tiled=True),
        lax.all_gather(merge_flat, "sp", axis=0, tiled=True),
    )
    projected = tuple(
        (jnp.dot(normed, weight_rows, preferred_element_type=jnp.float32) for weight_rows in pieces)
    )
    query_heads = w_query_window.shape[1] // HEAD
    group_heads = w_key_window.shape[1] // HEAD
    window_query = head_norm(projected[0], qk_gain[0], query_heads)
    window_key = head_norm(projected[1], qk_gain[1], group_heads)
    window_value = projected[2].astype(jnp.bfloat16).reshape(row_count, group_heads, HEAD)
    prev_key, prev_value = from_behind(
        (window_key[row_count - WINDOW :], window_value[row_count - WINDOW :]), "sp", 1
    )
    window_out = window_attend(
        window_query,
        jnp.concatenate([prev_key, window_key], axis=0),
        jnp.concatenate([prev_value, window_value], axis=0),
        sink_logits,
        row_offset,
    )
    forget_query = head_norm(projected[3], qk_gain[2], query_heads)
    forget_key = head_norm(projected[4], qk_gain[3], query_heads)
    forget_value = projected[5].astype(jnp.bfloat16).reshape(row_count, query_heads, HEAD)
    own_pos = row_offset + jnp.arange(row_count)
    forget_out = forget_groups(
        [(forget_query, gate_cum, own_pos)], forget_key, forget_value, gate_cum
    )[0]
    channel_count = w_merge.shape[2]
    merge_gate = jax.nn.sigmoid(projected[6]).reshape(row_count, 2, channel_count)
    branch_full = lax.all_gather(w_branch, "sp", axis=1, tiled=True)
    head_stack = jnp.stack([window_out, forget_out], axis=1)
    weight_rows = branch_full
    projection = jnp.einsum(
        "uxa,xag->uxg",
        lax.all_gather(head_stack, "tp", axis=2, tiled=True),
        weight_rows,
        preferred_element_type=jnp.float32,
    )
    return (merge_gate[:, 0] * projection[:, 0] + merge_gate[:, 1] * projection[:, 1]).astype(
        jnp.bfloat16
    )


def solution(mesh):
    return jax.shard_map(
        on_device,
        mesh=mesh,
        in_specs=(
            P(("grp", "sp"), "tp"),
            P(),
            P(),
            P("sp", "tp"),
            P("sp", "tp"),
            P("sp", "tp"),
            P("tp"),
            P("sp", "tp"),
            P("sp", "tp"),
            P("sp", "tp"),
            P(("grp", "sp"), "tp"),
            P("sp", None, "tp"),
            P(None, "sp", "tp"),
        ),
        out_specs=P(("grp", "sp"), "tp"),
        check_vma=False,
    )
```

profile of v0, /device:TPU:0, one launch (start us, length us, event | category | flops | bytes accessed | tf_op | source)
XLA Modules:
  0.0 339.6 jit_solution(14842164746860835694)
XLA Ops:
  13.7 16.6 %all_gather.48 = f32[1536,4]{0,1:T(4,128)} all-gather(f32[384,4]{0,1:T(4,128)} %param.27), channel_id=1, replica_groups=mesh['grp'=2,'sp'=4,'tp'=4] {'sp'}, dimensions={0}, use_global_device_ids=true | all-gather | bytes 30720 | tf_op jit(solution)/shard_map/all_gather | solution.py:76
  30.5 19.0 %all_gather.42 = bf16[2048,128]{1,0:T(8,128)(2,1)} all-gather(bf16[512,128]{1,0:T(8,128)(2,1)S(1)} %copy-done.8), channel_id=1, replica_groups=mesh['grp'=2,'sp'=4,'tp'=4] {'sp'}, dimensions={0}, use_global_device_ids=true | all-gather | bytes 655360 | tf_op jit(solution)/shard_map/all_gather | solution.py:175
  50.2 21.1 %all_gather.41 = bf16[2048,128]{1,0:T(8,128)(2,1)} all-gather(bf16[512,128]{1,0:T(8,128)(2,1)S(1)} %copy-done.9), channel_id=1, replica_groups=mesh['grp'=2,'sp'=4,'tp'=4] {'sp'}, dimensions={0}, use_global_device_ids=true | all-gather | bytes 655360 | tf_op jit(solution)/shard_map/all_gather | solution.py:176
  74.3 2.5 multiply_reduce_fusion.1
  77.0 25.4 %all_gather.45 = bf16[1536,4,64]{0,2,1:T(8,128)(2,1)S(1)} all-gather(bf16[384,4,64]{0,2,1:T(8,128)(2,1)S(1)} %multiply_convert_fusion.2), channel_id=1, replica_groups=mesh['grp'=2,'sp'=4,'tp'=4] {'sp'}, dimensions={0}, use_global_device_ids=true | all-gather | bytes 983040 | tf_op jit(solution)/shard_map/all_gather | solution.py:115
  102.5 5.3 %all-gather.17.cloned.1.call-done = bf16[2048,256]{1,0:T(8,128)(2,1)} async-done(((bf16[512,256]{1,0:T(8,128)(2,1)}), bf16[2048,256]{1,0:T(8,128)(2,1)}) %all-gather.17.cloned.1.call-update) | async-done | bytes 1048592 | tf_op jit(solution)/shard_map/all_gather | solution.py:179
  109.7 25.2 %all_gather.47 = bf16[1536,4,64]{0,2,1:T(8,128)(2,1)S(1)} all-gather(bf16[384,4,64]{0,2,1:T(8,128)(2,1)S(1)} %bitcast.165), channel_id=1, replica_groups=mesh['grp'=2,'sp'=4,'tp'=4] {'sp'}, dimensions={0}, use_global_device_ids=true | all-gather | bytes 983040 | tf_op jit(solution)/shard_map/all_gather | solution.py:116
  134.9 8.7 %all-gather.19.cloned.1.call-done = bf16[2048,256]{1,0:T(8,128)(2,1)} async-done(((bf16[512,256]{1,0:T(8,128)(2,1)}), bf16[2048,256]{1,0:T(8,128)(2,1)}) %all-gather.19.cloned.1.call-update) | async-done | bytes 1048592 | tf_op jit(solution)/shard_map/all_gather | solution.py:177
  149.0 35.5 %conditional.1 = (f32[4,384]{1,0:T(4,128)}, f32[384,4,64]{0,2,1:T(8,128)}) conditional(s32[]{:T(128)} %bitcast.13, () %tuple.20, (bf16[1536,4,64]{0,2,1:T(8,128)(2,1)S(1)}, bf16[1536,4,64]{0,2,1:T(8,128)(2,1)S(1)}, f32[1536,4]{0,1:T(4,128)}, s32[3,512]{1,0:T(4,128)S(1)}, s32[3,512]{1,0:T(4,128)S(1)}, /*index=5*/s32[384]{0:T(512)}, ...), branch_computations={%region_7.8_spmd, %region_8.13_spmd} | conditional | flops 215199744 | bytes 15060769 | solution.py:138
  151.0 33.5 %while.18 = (s32[]{:T(128)}, f32[4,384]{1,0:T(4,128)S(1)}, f32[4,384]{1,0:T(4,128)}, f32[384,4,64]{0,2,1:T(8,128)}, s32[384]{0:T(512)}, /*index=5*/s32[3,512]{1,...) while((s32[]{:T(128)}, f32[4,384]{1,0:T(4,128)S(1)}, ...), condition=%wide.region_12.12_spmd.clone, body=%wide.region_9.11_spmd.clone.sunk | while | flops 215196672 | bytes 11896481 | solution.py:133
  153.2 2.7 fusion.85
  158.8 2.7 fusion.89
  163.8 2.7 fusion.85
  170.1 2.9 fusion.89
  175.3 2.7 fusion.85
  181.6 2.9 fusion.89
  189.8 2.8 collective-permute-start.1
  192.6 3.3 collective-permute-start
  203.8 14.9 %all-gather.23.cloned.1.call-done = bf16[2,1024,512]{2,1,0:T(8,128)(2,1)} async-done(((bf16[2,256,512]{2,1,0:T(8,128)(2,1)}), bf16[2,1024,512]{2,1,0:T(8,128)(2,1)}) %all-gather.23.cloned.1.call-update) | async-done | bytes 2097168 | tf_op jit(solution)/shard_map/all_gather | solution.py:209
  218.6 21.5 %all-gather.21.cloned.1.call-done = bf16[384,2,1024]{2,0,1:T(8,128)(2,1)} async-done(((bf16[384,2,256]{2,0,1:T(8,128)(2,1)}), bf16[384,2,1024]{2,0,1:T(8,128)(2,1)}) %all-gather.21.cloned.1.call-update) | async-done | bytes 1572880 | tf_op jit(solution)/shard_map/all_gather | solution.py:214
  240.2 3.0 convolution_bitcast_fusion
  243.2 79.3 %all-gather.11.cloned.1.call-done = bf16[2048,1024]{1,0:T(8,128)(2,1)} async-done(((bf16[512,1024]{1,0:T(8,128)(2,1)}), bf16[2048,1024]{1,0:T(8,128)(2,1)}) %all-gather.11.cloned.1.call-update) | async-done | bytes 4194320 | tf_op jit(solution)/shard_map/all_gather | solution.py:180
  322.5 5.3 %add_divide_fusion = f32[384,1024]{1,0:T(8,128)} fusion(bf16[384,2048]{1,0:T(8,128)(2,1)S(1)} %copy-done.1, bf16[2048,1024]{1,0:T(8,128)(2,1)} %all-gather.11.cloned.1.call-done), kind=kOutput, calls=%fused_computation.44 | convolution fusion | flops 1611792384 | bytes 7340032 | tf_op jit(solution)/shard_map/dot_general | solution.py:183
  327.8 2.6 reshape.258
  (143 shorter events, 51.7 us)
Async XLA Ops:
  6.5 6.6 %copy-start.15 = (f32[4,64]{1,0:T(4,128)S(1)}, f32[4,64]{1,0:T(4,128)}, u32[]{:S(2)}) copy-start(f32[4,64]{1,0:T(4,128)} %param.19) | copy-start | bytes 3076
  6.5 24.0 %copy-start.8 = (bf16[512,128]{1,0:T(8,128)(2,1)S(1)}, bf16[512,128]{1,0:T(8,128)(2,1)}, u32[]{:S(2)}) copy-start(bf16[512,128]{1,0:T(8,128)(2,1)} %param.21) | copy-start | bytes 393220
  6.5 42.9 %copy-start.16 = (f32[4]{0:T(128)S(1)}, f32[4]{0:T(128)}, u32[]{:S(2)}) copy-start(f32[4]{0:T(128)} %param.23) | copy-start | bytes 52
  6.5 43.6 %copy-start.9 = (bf16[512,128]{1,0:T(8,128)(2,1)S(1)}, bf16[512,128]{1,0:T(8,128)(2,1)}, u32[]{:S(2)}) copy-start(bf16[512,128]{1,0:T(8,128)(2,1)} %param.22) | copy-start | bytes 393220
  6.5 65.4 %all-gather.9.cloned.1.call-start = ((), (), s32[]{:S(2)}) async-start(), calls=%async_computation | async-start | bytes 1966080 | tf_op jit(solution)/shard_map/all_gather | solution.py:165
  7.3 67.1 %all-gather.15.cloned.1.call-start = ((), (), s32[]{:S(2)}) async-start(), calls=%async_computation.3 | async-start | bytes 1310720 | tf_op jit(solution)/shard_map/all_gather | solution.py:178
  8.0 99.7 %all-gather.17.cloned.1.call-start = ((), (), s32[]{:S(2)}) async-start(), calls=%async_computation.4 | async-start | bytes 1310720 | tf_op jit(solution)/shard_map/all_gather | solution.py:179
  8.8 134.9 %all-gather.19.cloned.1.call-start = ((), (), s32[]{:S(2)}) async-start(), calls=%async_computation.5 | async-start | bytes 1310720 | tf_op jit(solution)/shard_map/all_gather | solution.py:177
  9.3 176.2 %all-gather.13.cloned.1.call-start = ((), (), s32[]{:S(2)}) async-start(), calls=%async_computation.2 | async-start | bytes 1310720 | tf_op jit(solution)/shard_map/all_gather | solution.py:174
  9.9 208.7 %all-gather.23.cloned.1.call-start = ((), (), s32[]{:S(2)}) async-start(), calls=%async_computation.7 | async-start | bytes 2621440 | tf_op jit(solution)/shard_map/all_gather | solution.py:209
  10.5 63.4 %copy-start.11 = (f32[2048]{0:T(1024)S(1)}, f32[2048]{0:T(1024)}, u32[]{:S(2)}) copy-start(f32[2048]{0:T(1024)} %param.18) | copy-start | bytes 24580
  10.5 229.6 %all-gather.21.cloned.1.call-start = ((), (), s32[]{:S(2)}) async-start(), calls=%async_computation.6 | async-start | bytes 1966080 | tf_op jit(solution)/shard_map/all_gather | solution.py:214
  71.9 1.9 copy-start.2
  74.3 72.6 %copy-start = (bf16[384,2048]{1,0:T(8,128)(2,1)}, bf16[384,2048]{1,0:T(8,128)(2,1)S(1)}, u32[]{:S(2)}) copy-start(bf16[384,2048]{1,0:T(8,128)(2,1)S(1)} %fusion.27) | copy-start | bytes 4718596
  143.7 2.1 copy-start.3
  145.7 1.2 copy-start.4
  185.5 2.6 copy-start.5
  188.4 1.2 copy-start.12
  188.6 7.3 %copy-start.14 = (f32[64]{0:T(128)S(1)}, f32[64]{0:T(128)}, u32[]{:S(2)}) copy-start(f32[64]{0:T(128)} %get-tuple-element.195) | copy-start | bytes 772
  189.8 7.2 %collective-permute-start.1 = (bf16[128,2,64]{0,2,1:T(8,128)(2,1)S(1)}, bf16[128,2,64]{0,2,1:T(8,128)(2,1)S(1)}, u32[]{:S(2)}, u32[]{:S(2)}) collective-permute-start(bf16[128,2,64]{0,2,1:T(8,128)(2,1)S(1)} %slice.68), channel_id=1, source_target_pairs={{0,4},{4,8},{8,12},{1,5},{5,9},{9,13},{2,6},{6,10},{10,14},{3,7},{... | collective-permute-start | bytes 98312 | tf_op jit(solution)/shard_map/ppermute | solution.py:16
  192.6 5.4 %collective-permute-start = (bf16[128,2,64]{0,2,1:T(8,128)(2,1)S(1)}, bf16[128,2,64]{0,2,1:T(8,128)(2,1)S(1)}, u32[]{:S(2)}, u32[]{:S(2)}) collective-permute-start(bf16[128,2,64]{0,2,1:T(8,128)(2,1)S(1)} %bitcast.167), channel_id=1, source_target_pairs={{0,4},{4,8},{8,12},{1,5},{5,9},{9,13},{2,6},{6,10},{10,14},{3,7},{... | collective-permute-start | bytes 98312 | tf_op jit(solution)/shard_map/ppermute | solution.py:16
  200.9 1.5 copy-start.6
  202.4 120.1 %all-gather.11.cloned.1.call-start = ((), (), s32[]{:S(2)}) async-start(), calls=%async_computation.1 | async-start | bytes 5242880 | tf_op jit(solution)/shard_map/all_gather | solution.py:180
  203.8 118.7 %copy-start.1 = (bf16[384,2048]{1,0:T(8,128)(2,1)S(1)}, bf16[384,2048]{1,0:T(8,128)(2,1)}, u32[]{:S(2)}) copy-start(bf16[384,2048]{1,0:T(8,128)(2,1)} %copy-done) | copy-start | bytes 4718596
  (3 other events, 3.0 us)
Sparse Core Ops, SparseCore 0:
  8.9 22.3 all-gather.8
  32.9 36.9 all-gather.14
  71.5 36.1 all-gather.16
  109.1 34.4 all-gather.18
  145.1 27.0 all-gather.12
  173.6 45.0 all-gather.22
  220.2 19.9 all-gather.20
  241.7 80.7 all-gather.10
where the time goes:
time: 341 us; the launch traced here: 340 us
  waiting for transfers between devices  134 us (39%)
  blocking collectives  107 us (31%)
  matrix products  37.9 us (11%)
  other arithmetic  23.1 us (7%)
  local copies, waits for them, and re-layouts  16.3 us (5%)
  between operations  14.7 us (4%)
  starting transfers between devices  6.38 us (2%)
    all_gather x1, waiting for transfers between devices, on_device(): lax.all_gather(merge_flat, 'sp', axis=0, tiled=True)  79.3 us
    all_gather x1, blocking collectives, forget_groups(): key_rows = lax.all_gather(keys, 'sp', axis=0, tiled=True)  25.4 us
    all_gather x1, blocking collectives, forget_groups(): value_rows = lax.all_gather(values, 'sp', axis=0, tiled=True)  25.2 us
    all_gather x1, waiting for transfers between devices, on_device(): lax.all_gather(head_stack, 'tp', axis=2, tiled=True)  21.5 us
    all_gather x1, blocking collectives, on_device(): lax.all_gather(w_value_window, 'sp', axis=0, tiled=True)  21.1 us
    all_gather x1, blocking collectives, on_device(): lax.all_gather(w_key_window, 'sp', axis=0, tiled=True)  19 us
    dot_general x7, matrix products, on_device(): jnp.dot(normed, weight_rows, preferred_element_type=jnp.float32)  16.8 us
    all_gather x1, blocking collectives, forget_groups(): gates_all = lax.all_gather(gates, 'sp', axis=0, tiled=True)  16.6 us
  transfers between devices with their start and end apart: 10, of which 6 were waited for; matrix products, arithmetic and copies ran while one was open for 20% of the time, Pallas kernels for 0%

commit v1 on v0

--- a/solution.py
+++ b/solution.py
@@ -209,12 +209,37 @@
     branch_full = lax.all_gather(w_branch, "sp", axis=1, tiled=True)
     head_stack = jnp.stack([window_out, forget_out], axis=1)
     weight_rows = branch_full
+    count, index, extent = (lax.axis_size("tp"), lax.axis_index("tp"), head_stack.shape[2])
+    right = [(i_2, (i_2 + 1) % count) for i_2 in range(count)]
+    left = [(i_2, (i_2 - 1) % count) for i_2 in range(count)]
+    half = count // 2
+    from_left = from_right = head_stack
     projection = jnp.einsum(
         "uxa,xag->uxg",
-        lax.all_gather(head_stack, "tp", axis=2, tiled=True),
-        weight_rows,
+        head_stack,
+        lax.dynamic_slice_in_dim(weight_rows, index * extent, head_stack.shape[2], axis=1),
         preferred_element_type=jnp.float32,
     )
+    for step in range(1, half + 1):
+        from_left = lax.ppermute(from_left, "tp", right)
+        if step < count - half:
+            from_right = lax.ppermute(from_right, "tp", left)
+            projection = projection + jnp.einsum(
+                "uxa,xag->uxg",
+                from_right,
+                lax.dynamic_slice_in_dim(
+                    weight_rows, (index + step) % count * extent, from_right.shape[2], axis=1
+                ),
+                preferred_element_type=jnp.float32,
+            )
+        projection = projection + jnp.einsum(
+            "uxa,xag->uxg",
+            from_left,
+            lax.dynamic_slice_in_dim(
+                weight_rows, (index - step) % count * extent, from_left.shape[2], axis=1
+            ),
+            preferred_element_type=jnp.float32,
+        )
     return (merge_gate[:, 0] * projection[:, 0] + merge_gate[:, 1] * projection[:, 1]).astype(
         jnp.bfloat16
     )

time: 341 us -> 317 us (0.930)
  waiting for transfers between devices: 134 us -> 102 us
  local copies, waits for them, and re-layouts: 16.3 us -> 21.9 us
    all_gather x1 -> x0, waiting for transfers between devices: 21.5 us -> none  [on_device(): lax.all_gather(head_stack, 'tp', axis=2, tiled=True)]
    all_gather x1, waiting for transfers between devices: 79.3 us -> 58 us  [on_device(): lax.all_gather(merge_flat, 'sp', axis=0, tiled=True)]
    all_gather x1, waiting for transfers between devices: 5.25 us -> 23.9 us  [on_device(): lax.all_gather(w_value_forget, 'sp', axis=0, tiled=True)]
    all_gather x1, waiting for transfers between devices: 14.9 us -> 0.01 us  [on_device(): branch_full = lax.all_gather(w_branch, 'sp', axis=1, tiled=True)]
    ppermute x0 -> x3, waiting for transfers between devices: none -> 12.4 us  [the longest x2 12.4 us: on_device(): from_left = lax.ppermute(from_left, 'tp', right)]
    all_gather x1, waiting for transfers between devices: 8.71 us -> 4 us  [on_device(): lax.all_gather(w_query_forget, 'sp', axis=0, tiled=True)]
  transfers between devices with their start and end apart: 10 -> 12, of which waited for: 6 -> 5; matrix products, arithmetic and copies ran while one was open for 20% -> 24% of each run, Pallas kernels for 0% -> 0%
where the time goes in v1:
time: 317 us; the launch traced here: 316 us
  blocking collectives  107 us (34%)
  waiting for transfers between devices  102 us (32%)
  matrix products  38.4 us (12%)
  other arithmetic  23.7 us (7%)
  local copies, waits for them, and re-layouts  21.9 us (7%)
  between operations  14.7 us (5%)
  starting transfers between devices  8.58 us (3%)
    all_gather x1, waiting for transfers between devices, on_device(): lax.all_gather(merge_flat, 'sp', axis=0, tiled=True)  58 us
    all_gather x1, blocking collectives, forget_groups(): key_rows = lax.all_gather(keys, 'sp', axis=0, tiled=True)  26.3 us
    all_gather x1, blocking collectives, forget_groups(): value_rows = lax.all_gather(values, 'sp', axis=0, tiled=True)  24.5 us
    all_gather x1, waiting for transfers between devices, on_device(): lax.all_gather(w_value_forget, 'sp', axis=0, tiled=True)  23.9 us
    all_gather x1, blocking collectives, on_device(): lax.all_gather(w_value_window, 'sp', axis=0, tiled=True)  20.1 us
    all_gather x1, blocking collectives, on_device(): lax.all_gather(w_key_window, 'sp', axis=0, tiled=True)  19.3 us
    all_gather x1, blocking collectives, forget_groups(): gates_all = lax.all_gather(gates, 'sp', axis=0, tiled=True)  16.6 us
    dot_general x7, matrix products, on_device(): jnp.dot(normed, weight_rows, preferred_element_type=jnp.float32)  15.4 us
  transfers between devices with their start and end apart: 12, of which 5 were waited for; matrix products, arithmetic and copies ran while one was open for 24% of the time, Pallas kernels for 0%

profile of v1, /device:TPU:0, one launch (start us, length us, event | category | flops | bytes accessed | tf_op | source)
XLA Modules:
  0.0 315.7 jit_solution(14214364911437549301)
XLA Ops:
  15.6 16.6 %all_gather.46 = f32[1536,4]{0,1:T(4,128)} all-gather(f32[384,4]{0,1:T(4,128)} %param.27), channel_id=1, replica_groups=mesh['grp'=2,'sp'=4,'tp'=4] {'sp'}, dimensions={0}, use_global_device_ids=true | all-gather | bytes 30720 | tf_op jit(solution)/shard_map/all_gather | solution.py:76
  32.4 19.3 %all_gather.40 = bf16[2048,128]{1,0:T(8,128)(2,1)} all-gather(bf16[512,128]{1,0:T(8,128)(2,1)S(1)} %copy-done.9), channel_id=1, replica_groups=mesh['grp'=2,'sp'=4,'tp'=4] {'sp'}, dimensions={0}, use_global_device_ids=true | all-gather | bytes 655360 | tf_op jit(solution)/shard_map/all_gather | solution.py:175
  52.4 20.1 %all_gather.39 = bf16[2048,128]{1,0:T(8,128)(2,1)S(1)} all-gather(bf16[512,128]{1,0:T(8,128)(2,1)S(1)} %copy-done.10), channel_id=1, replica_groups=mesh['grp'=2,'sp'=4,'tp'=4] {'sp'}, dimensions={0}, use_global_device_ids=true | all-gather | bytes 655360 | tf_op jit(solution)/shard_map/all_gather | solution.py:176
  75.0 2.5 multiply_reduce_fusion.1
  77.6 26.3 %all_gather.43 = bf16[1536,4,64]{0,2,1:T(8,128)(2,1)S(1)} all-gather(bf16[384,4,64]{0,2,1:T(8,128)(2,1)S(1)} %multiply_convert_fusion.2), channel_id=1, replica_groups=mesh['grp'=2,'sp'=4,'tp'=4] {'sp'}, dimensions={0}, use_global_device_ids=true | all-gather | bytes 983040 | tf_op jit(solution)/shard_map/all_gather | solution.py:115
  103.9 4.0 %all-gather.20.cloned.1.call-done = bf16[2048,256]{1,0:T(8,128)(2,1)} async-done(((bf16[512,256]{1,0:T(8,128)(2,1)}), bf16[2048,256]{1,0:T(8,128)(2,1)}) %all-gather.20.cloned.1.call-update) | async-done | bytes 1048592 | tf_op jit(solution)/shard_map/all_gather | solution.py:177
  112.8 23.9 %all-gather.18.cloned.1.call-done = bf16[2048,256]{1,0:T(8,128)(2,1)} async-done(((bf16[512,256]{1,0:T(8,128)(2,1)}), bf16[2048,256]{1,0:T(8,128)(2,1)}) %all-gather.18.cloned.1.call-update) | async-done | bytes 1048592 | tf_op jit(solution)/shard_map/all_gather | solution.py:179
  138.6 24.5 %all_gather.45 = bf16[1536,4,64]{0,2,1:T(8,128)(2,1)S(1)} all-gather(bf16[384,4,64]{0,2,1:T(8,128)(2,1)S(1)} %bitcast.168), channel_id=1, replica_groups=mesh['grp'=2,'sp'=4,'tp'=4] {'sp'}, dimensions={0}, use_global_device_ids=true | all-gather | bytes 983040 | tf_op jit(solution)/shard_map/all_gather | solution.py:116
  163.1 35.5 %conditional.1 = (f32[4,384]{1,0:T(4,128)}, f32[384,4,64]{0,2,1:T(8,128)}) conditional(s32[]{:T(128)} %bitcast.13, () %tuple.20, (bf16[1536,4,64]{0,2,1:T(8,128)(2,1)S(1)}, bf16[1536,4,64]{0,2,1:T(8,128)(2,1)S(1)}, f32[1536,4]{0,1:T(4,128)}, s32[3,512]{1,0:T(4,128)S(1)}, s32[3,512]{1,0:T(4,128)S(1)}, /*index=5*/s32[384]{0:T(512)}, ...), branch_computations={%region_7.8_spmd, %region_8.13_spmd} | conditional | flops 215199744 | bytes 15060769 | solution.py:138
  165.1 33.5 %while.18 = (s32[]{:T(128)}, f32[4,384]{1,0:T(4,128)S(1)}, f32[4,384]{1,0:T(4,128)}, f32[384,4,64]{0,2,1:T(8,128)}, s32[384]{0:T(512)}, /*index=5*/s32[3,512]{1,...) while((s32[]{:T(128)}, f32[4,384]{1,0:T(4,128)S(1)}, ...), condition=%wide.region_12.12_spmd.clone, body=%wide.region_9.11_spmd.clone.sunk | while | flops 215196672 | bytes 11896481 | solution.py:133
  167.3 2.7 fusion.96
  173.0 2.7 fusion.100
  178.0 2.7 fusion.96
  184.3 2.9 fusion.100
  189.4 2.7 fusion.96
  195.7 2.9 fusion.100
  199.8 2.5 bitcast_reduce_fusion
  206.7 3.6 %collective-permute-start.1 = (bf16[128,2,64]{0,2,1:T(8,128)(2,1)S(1)}, bf16[128,2,64]{0,2,1:T(8,128)(2,1)S(1)}, u32[]{:S(2)}, u32[]{:S(2)}) collective-permute-start(bf16[128,2,64]{0,2,1:T(8,128)(2,1)S(1)} %slice.68), channel_id=1, source_target_pairs={{0,4},{4,8},{8,12},{1,5},{5,9},{9,13},{2,6},{6,10},{10,14},{3,7},{... | collective-permute-start | bytes 98312 | tf_op jit(solution)/shard_map/ppermute | solution.py:16
  211.2 2.9 collective-permute-start
  214.2 2.6 multiply_convert_fusion
  225.9 7.9 %collective-permute-done.3 = bf16[384,2,256]{2,0,1:T(8,128)(2,1)S(1)} collective-permute-done((bf16[384,2,256]{2,0,1:T(8,128)(2,1)S(1)}, bf16[384,2,256]{2,0,1:T(8,128)(2,1)S(1)}, u32[]{:S(2)}, u32[]{:S(2)}) %collective-permute-start.3) | collective-permute-done | bytes 393248 | tf_op jit(solution)/shard_map/ppermute | solution.py:224
  236.6 4.5 %collective-permute-done.4 = bf16[384,2,256]{2,0,1:T(8,128)(2,1)} collective-permute-done((bf16[384,2,256]{2,0,1:T(8,128)(2,1)S(1)}, bf16[384,2,256]{2,0,1:T(8,128)(2,1)}, u32[]{:S(2)}, u32[]{:S(2)}) %collective-permute-start.4) | collective-permute-done | bytes 393248 | tf_op jit(solution)/shard_map/ppermute | solution.py:224
  242.5 58.0 %all-gather.10.cloned.1.call-done = bf16[2048,1024]{1,0:T(8,128)(2,1)} async-done(((bf16[512,1024]{1,0:T(8,128)(2,1)}), bf16[2048,1024]{1,0:T(8,128)(2,1)}) %all-gather.10.cloned.1.call-update) | async-done | bytes 4194320 | tf_op jit(solution)/shard_map/all_gather | solution.py:180
  300.6 5.3 %add_divide_fusion = f32[384,1024]{1,0:T(8,128)} fusion(bf16[384,2048]{1,0:T(8,128)(2,1)S(1)} %copy-done.1, bf16[2048,1024]{1,0:T(8,128)(2,1)} %all-gather.10.cloned.1.call-done), kind=kOutput, calls=%fused_computation.45 | convolution fusion | flops 1611792384 | bytes 7340032 | tf_op jit(solution)/shard_map/dot_general | solution.py:183
  (148 shorter events, 60.0 us)
Async XLA Ops:
  6.5 3.4 %copy-start.6 = (bf16[2,256,512]{2,1,0:T(8,128)(2,1)S(1)}, bf16[2,256,512]{2,1,0:T(8,128)(2,1)}, u32[]{:S(2)}) copy-start(bf16[2,256,512]{2,1,0:T(8,128)(2,1)} %param.29) | copy-start | bytes 1572868
  6.5 4.5 %copy-start.5 = (bf16[512,2,512]{2,1,0:T(2,128)(2,1)S(1)}, bf16[512,2,512]{2,1,0:T(2,128)(2,1)}, u32[]{:S(2)}) copy-start(bf16[512,2,512]{2,1,0:T(2,128)(2,1)} %param.28) | copy-start | bytes 3145732
  6.5 66.0 %all-gather.8.cloned.1.call-start = ((), (), s32[]{:S(2)}) async-start(), calls=%async_computation | async-start | bytes 1966080 | tf_op jit(solution)/shard_map/all_gather | solution.py:165
  7.3 67.7 %all-gather.16.cloned.1.call-start = ((), (), s32[]{:S(2)}) async-start(), calls=%async_computation.4 | async-start | bytes 1310720 | tf_op jit(solution)/shard_map/all_gather | solution.py:178
  8.0 99.9 %all-gather.20.cloned.1.call-start = ((), (), s32[]{:S(2)}) async-start(), calls=%async_computation.6 | async-start | bytes 1310720 | tf_op jit(solution)/shard_map/all_gather | solution.py:177
  8.7 127.9 %all-gather.18.cloned.1.call-start = ((), (), s32[]{:S(2)}) async-start(), calls=%async_computation.5 | async-start | bytes 1310720 | tf_op jit(solution)/shard_map/all_gather | solution.py:179
  9.3 190.5 %all-gather.14.cloned.1.call-start = ((), (), s32[]{:S(2)}) async-start(), calls=%async_computation.3 | async-start | bytes 1310720 | tf_op jit(solution)/shard_map/all_gather | solution.py:174
  9.9 224.0 %all-gather.12.cloned.1.call-start = ((), (), s32[]{:S(2)}) async-start(), calls=%async_computation.2 | async-start | bytes 2621440 | tf_op jit(solution)/shard_map/all_gather | solution.py:209
  11.0 289.6 %all-gather.10.cloned.1.call-start = ((), (), s32[]{:S(2)}) async-start(), calls=%async_computation.1 | async-start | bytes 5242880 | tf_op jit(solution)/shard_map/all_gather | solution.py:180
  11.0 3.9 %copy-start.14 = (f32[4,64]{1,0:T(4,128)S(1)}, f32[4,64]{1,0:T(4,128)}, u32[]{:S(2)}) copy-start(f32[4,64]{1,0:T(4,128)} %param.19) | copy-start | bytes 3076
  11.1 21.3 %copy-start.9 = (bf16[512,128]{1,0:T(8,128)(2,1)S(1)}, bf16[512,128]{1,0:T(8,128)(2,1)}, u32[]{:S(2)}) copy-start(bf16[512,128]{1,0:T(8,128)(2,1)} %param.21) | copy-start | bytes 393220
  11.1 40.6 %copy-start.15 = (f32[4]{0:T(128)S(1)}, f32[4]{0:T(128)}, u32[]{:S(2)}) copy-start(f32[4]{0:T(128)} %param.23) | copy-start | bytes 52
  11.1 41.3 %copy-start.10 = (bf16[512,128]{1,0:T(8,128)(2,1)S(1)}, bf16[512,128]{1,0:T(8,128)(2,1)}, u32[]{:S(2)}) copy-start(bf16[512,128]{1,0:T(8,128)(2,1)} %param.22) | copy-start | bytes 393220
  12.4 62.0 %copy-start.11 = (f32[2048]{0:T(1024)S(1)}, f32[2048]{0:T(1024)}, u32[]{:S(2)}) copy-start(f32[2048]{0:T(1024)} %param.18) | copy-start | bytes 24580
  72.5 1.9 copy-start.2
  74.9 61.7 %copy-start = (bf16[384,2048]{1,0:T(8,128)(2,1)}, bf16[384,2048]{1,0:T(8,128)(2,1)S(1)}, u32[]{:S(2)}) copy-start(bf16[384,2048]{1,0:T(8,128)(2,1)S(1)} %fusion.27) | copy-start | bytes 4718596
  202.3 3.5 %copy-start.1 = (bf16[384,2048]{1,0:T(8,128)(2,1)S(1)}, bf16[384,2048]{1,0:T(8,128)(2,1)}, u32[]{:S(2)}) copy-start(bf16[384,2048]{1,0:T(8,128)(2,1)} %copy-done) | copy-start | bytes 4718596
  202.3 3.4 %copy-start.3 = (bf16[2048,128]{1,0:T(8,128)(2,1)S(1)}, bf16[2048,128]{1,0:T(8,128)(2,1)}, u32[]{:S(2)}) copy-start(bf16[2048,128]{1,0:T(8,128)(2,1)} %all_gather.40) | copy-start | bytes 1572868
  206.7 11.5 %collective-permute-start.1 = (bf16[128,2,64]{0,2,1:T(8,128)(2,1)S(1)}, bf16[128,2,64]{0,2,1:T(8,128)(2,1)S(1)}, u32[]{:S(2)}, u32[]{:S(2)}) collective-permute-start(bf16[128,2,64]{0,2,1:T(8,128)(2,1)S(1)} %slice.68), channel_id=1, source_target_pairs={{0,4},{4,8},{8,12},{1,5},{5,9},{9,13},{2,6},{6,10},{10,14},{3,7},{... | collective-permute-start | bytes 98312 | tf_op jit(solution)/shard_map/ppermute | solution.py:16
  211.2 7.5 %collective-permute-start = (bf16[128,2,64]{0,2,1:T(8,128)(2,1)}, bf16[128,2,64]{0,2,1:T(8,128)(2,1)S(1)}, u32[]{:S(2)}, u32[]{:S(2)}) collective-permute-start(bf16[128,2,64]{0,2,1:T(8,128)(2,1)} %bitcast.170), channel_id=1, source_target_pairs={{0,4},{4,8},{8,12},{1,5},{5,9},{9,13},{2,6},{6,10},{10,14},{3,7},{... | collective-permute-start | bytes 98312 | tf_op jit(solution)/shard_map/ppermute | solution.py:16
  224.1 9.7 %collective-permute-start.3 = (bf16[384,2,256]{2,0,1:T(8,128)(2,1)S(1)}, bf16[384,2,256]{2,0,1:T(8,128)(2,1)S(1)}, u32[]{:S(2)}, u32[]{:S(2)}) collective-permute-start(bf16[384,2,256]{2,0,1:T(8,128)(2,1)S(1)} %pad_maximum_fusion), channel_id=1, source_target_pairs={{0,1},{1,2},{2,3},{3,0},{4,5},{5,6},{6,7},{7,4},{8,9},{9,10},{10,1... | collective-permute-start | bytes 1179656 | tf_op jit(solution)/shard_map/ppermute | solution.py:224
  224.2 11.9 %collective-permute-start.2 = (bf16[384,2,256]{2,0,1:T(8,128)(2,1)S(1)}, bf16[384,2,256]{2,0,1:T(8,128)(2,1)S(1)}, u32[]{:S(2)}, u32[]{:S(2)}) collective-permute-start(bf16[384,2,256]{2,0,1:T(8,128)(2,1)S(1)} %pad_maximum_fusion), channel_id=1, source_target_pairs={{0,3},{1,0},{2,1},{3,2},{4,7},{5,4},{6,5},{7,6},{8,11},{9,8},{10,9... | collective-permute-start | bytes 1179656 | tf_op jit(solution)/shard_map/ppermute | solution.py:226
  233.8 7.3 %collective-permute-start.4 = (bf16[384,2,256]{2,0,1:T(8,128)(2,1)S(1)}, bf16[384,2,256]{2,0,1:T(8,128)(2,1)}, u32[]{:S(2)}, u32[]{:S(2)}) collective-permute-start(bf16[384,2,256]{2,0,1:T(8,128)(2,1)S(1)} %collective-permute-done.3), channel_id=1, source_target_pairs={{0,1},{1,2},{2,3},{3,0},{4,5},{5,6},{6,7},{7,4},{8,9},{9,10},{10,1... | collective-permute-start | bytes 1179656 | tf_op jit(solution)/shard_map/ppermute | solution.py:224
  233.9 1.8 copy-start.4
  (4 other events, 4.8 us)
Sparse Core Ops, SparseCore 0:
  8.9 22.3 all-gather.7
  32.8 37.7 all-gather.15
  72.3 35.5 all-gather.19
  109.3 27.2 all-gather.17
  138.1 34.2 all-gather.13
  173.7 45.2 all-gather.11
  220.7 79.8 all-gather.9
